TPU v7x, 32 devices: a whole 2x2x4 slice. The times are simulated.
32 devices in a mesh: rep: 2 (over x), fs: 4 (over z), tp: 4 (over y, core).
Axes of the slice: x: 2, y: 2, z: 4, core: 2. Of those that a mesh axis runs over, the one named last changes fastest.
Arguments:
- tokens: bfloat16 [8192, 2048], P(('rep', 'fs'), 'tp'), may hold values from -6 to 6
- mix_in_gain: bfloat16 [2048], replicated, may hold values from 0.099609375 to 1.8984375
- bgate_weight: bfloat16 [2048, 2048], P('fs', 'tp'), may hold values from -0.125 to 0.125
- cgate_weight: bfloat16 [2048, 2048], P('fs', 'tp'), may hold values from -0.125 to 0.125
- value_weight: bfloat16 [2048, 2048], P('fs', 'tp'), may hold values from -0.125 to 0.125
- conv_taps: bfloat16 [3, 2048], replicated, may hold values from -3 to 3
- out_weight: bfloat16 [2048, 2048], P('tp', 'fs'), may hold values from -0.41984465 to 0.41984465
- mix_out_gain: bfloat16 [2048], replicated, may hold values from 0.099609375 to 1.8984375
- ffn_in_gain: bfloat16 [2048], replicated, may hold values from 0.099609375 to 1.8984375
- up_weight: bfloat16 [2048, 8192], P('fs', 'tp'), may hold values from -0.125 to 0.125
- down_weight: bfloat16 [8192, 2048], P('tp', 'fs'), may hold values from -0.20992233 to 0.20992233
- ffn_out_gain: bfloat16 [2048], replicated, may hold values from 0.099609375 to 1.8984375
Outputs:
- result: bfloat16 [8192, 2048], P(('rep', 'fs'), 'tp')
All inputs are finite; a program needn't handle non-finite values.
Results may differ from a plain program's by a relative error of at most 0.02.
Values may be sent and summed in bfloat16 or wider, within the bound.
A program may use at most 128 MiB of HBM per device.

v0:
```python
import jax
import jax.numpy as jnp
from jax import lax
from jax.sharding import PartitionSpec as P

LEN = 256
epsilon = 1e-06


def normalize(rows, gain):
    rows = rows.astype(jnp.float32)
    factor = lax.rsqrt(jnp.mean(rows * rows, axis=-1, keepdims=True) + epsilon)
    return rows * factor * gain.astype(jnp.float32)


def convolve(inner, taps):
    seqs = inner.reshape(-1, LEN, inner.shape[1])
    padded = jnp.pad(seqs, ((0, 0), (1, 1), (0, 0)))
    weights = taps.astype(jnp.float32)
    out = weights[0] * padded[:, :-2] + weights[1] * padded[:, 1:-1] + weights[2] * padded[:, 2:]
    return out.reshape(inner.shape)


def body(
    tokens,
    mix_in_gain,
    bgate_weight,
    cgate_weight,
    value_weight,
    conv_taps,
    out_weight,
    mix_out_gain,
    ffn_in_gain,
    up_weight,
    down_weight,
    ffn_out_gain,
):
    column = lax.axis_index("tp")
    own_width = tokens.shape[1]
    first = column * own_width
    full_width = mix_in_gain.shape[0]
    whole = lax.all_gather(tokens, "tp", axis=1, tiled=True)
    normed = normalize(whole, mix_in_gain).astype(jnp.bfloat16)

    def add_rows(piece):
        return jnp.dot(normed, piece, preferred_element_type=jnp.float32)

    bgate = add_rows(lax.all_gather(bgate_weight, "fs", axis=0, tiled=True))
    cgate = add_rows(lax.all_gather(cgate_weight, "fs", axis=0, tiled=True))
    value = add_rows(lax.all_gather(value_weight, "fs", axis=0, tiled=True))
    bgate = bgate.astype(jnp.bfloat16)
    cgate = cgate.astype(jnp.bfloat16)
    value = value.astype(jnp.bfloat16)
    channels = bgate.shape[1]
    own_taps = lax.dynamic_slice_in_dim(conv_taps, column * channels, channels, 1)
    inner = cgate.astype(jnp.float32) * value.astype(jnp.float32)
    gated = (bgate.astype(jnp.float32) * convolve(inner, own_taps)).astype(jnp.bfloat16)
    partial_mix = jnp.dot(
        gated,
        lax.all_gather(out_weight, "fs", axis=1, tiled=True),
        preferred_element_type=jnp.float32,
    )
    mixed = lax.psum(partial_mix.astype(jnp.bfloat16), "tp").astype(jnp.float32)
    resid = (whole.astype(jnp.float32) + normalize(mixed, mix_out_gain)).astype(jnp.bfloat16)
    resid_own = lax.dynamic_slice_in_dim(resid, first, own_width, 1)
    second = normalize(resid, ffn_in_gain).astype(jnp.bfloat16)
    lifted = jnp.dot(
        second,
        lax.all_gather(up_weight, "fs", axis=0, tiled=True),
        preferred_element_type=jnp.float32,
    )
    active = jnp.square(jnp.maximum(lifted, 0.0)).astype(jnp.bfloat16)
    partial_ffn = jnp.dot(
        active,
        lax.all_gather(down_weight, "fs", axis=1, tiled=True),
        preferred_element_type=jnp.float32,
    )
    ffn = lax.psum_scatter(
        partial_ffn.astype(jnp.bfloat16), "tp", scatter_dimension=1, tiled=True
    ).astype(jnp.float32)
    ffn_energy = lax.psum(jnp.sum(ffn * ffn, axis=1), "tp")
    out_gain = lax.dynamic_slice_in_dim(ffn_out_gain, first, own_width, 0).astype(jnp.float32)
    closing = ffn * lax.rsqrt(ffn_energy[:, None] / full_width + epsilon) * out_gain
    return (resid_own.astype(jnp.float32) + closing).astype(jnp.bfloat16)


def solution(mesh):
    placed = (
        P(("rep", "fs"), "tp"),
        P(),
        P("fs", "tp"),
        P("fs", "tp"),
        P("fs", "tp"),
        P(),
        P("tp", "fs"),
        P(),
        P(),
        P("fs", "tp"),
        P("tp", "fs"),
        P(),
    )
    return jax.shard_map(
        body, mesh=mesh, in_specs=placed, out_specs=P(("rep", "fs"), "tp"), check_vma=False
    )
```

profile of v0, /device:TPU:0, one launch (start us, length us, event | category | flops | bytes accessed | tf_op | source)
XLA Modules:
  0.0 707.6 jit_solution(8818610116150277627)
XLA Ops:
  6.5 0.0 all-gather.8.cloned.1.call-start
  6.5 0.7 all-gather.8.cloned.1.call-update
  7.3 0.0 all-gather.12.cloned.1.call-start
  7.3 0.7 all-gather.12.cloned.1.call-update
  8.0 0.0 all-gather.14.cloned.1.call-start
  8.1 0.7 all-gather.14.cloned.1.call-update
  8.7 0.0 all-gather.10.cloned.1.call-start
  8.8 0.5 all-gather.10.cloned.1.call-update
  9.3 0.0 all-gather.16.cloned.1.call-start
  9.4 0.5 all-gather.16.cloned.1.call-update
  9.9 0.0 all-reduce.3.cloned.1.call-start
  10.0 0.7 dynamic-slice_convert_fusion
  10.7 0.7 convert_element_type.76
  11.4 34.8 %all-gather.8.cloned.1.call-done = bf16[1024,2048]{1,0:T(8,128)(2,1)} async-done(((bf16[1024,512]{1,0:T(8,128)(2,1)}), bf16[1024,2048]{1,0:T(8,128)(2,1)}) %all-gather.8.cloned.1.call-update) | async-done | bytes 4194320 | tf_op jit(solution)/shard_map/all_gather | solution.py:42
  46.1 3.1 fusion.5
  49.2 44.2 %all-gather.12.cloned.1.call-done = bf16[2048,512]{1,0:T(8,128)(2,1)} async-done(((bf16[512,512]{1,0:T(8,128)(2,1)}), bf16[2048,512]{1,0:T(8,128)(2,1)}) %all-gather.12.cloned.1.call-update) | async-done | bytes 2097168 | tf_op jit(solution)/shard_map/all_gather | solution.py:49
  93.4 5.2 convolution_convert_fusion.2
  98.6 40.8 %all-gather.14.cloned.1.call-done = bf16[2048,512]{1,0:T(8,128)(2,1)} async-done(((bf16[512,512]{1,0:T(8,128)(2,1)}), bf16[2048,512]{1,0:T(8,128)(2,1)}) %all-gather.14.cloned.1.call-update) | async-done | bytes 2097168 | tf_op jit(solution)/shard_map/all_gather | solution.py:50
  139.4 5.2 convert_multiply_fusion.8
  144.7 0.6 multiply_add_fusion
  145.3 40.0 %all-gather.10.cloned.1.call-done = bf16[2048,512]{1,0:T(8,128)(2,1)} async-done(((bf16[512,512]{1,0:T(8,128)(2,1)}), bf16[2048,512]{1,0:T(8,128)(2,1)}) %all-gather.10.cloned.1.call-update) | async-done | bytes 2097168 | tf_op jit(solution)/shard_map/all_gather | solution.py:48
  185.4 5.2 fusion.25
  190.6 40.7 %all-gather.16.cloned.1.call-done = bf16[512,2048]{1,0:T(8,128)(2,1)} async-done(((bf16[512,512]{1,0:T(8,128)(2,1)}), bf16[512,2048]{1,0:T(8,128)(2,1)}) %all-gather.16.cloned.1.call-update) | async-done | bytes 2097168 | tf_op jit(solution)/shard_map/all_gather | solution.py:60
  231.3 5.9 convolution_convert_fusion
  237.2 0.0 copy-start.1
  237.2 0.0 copy-start.2
  237.2 0.0 all-reduce.3.cloned.1.call-update
  237.2 0.0 all-gather.18.cloned.1.call-start
  237.2 0.7 all-gather.18.cloned.1.call-update
  237.9 0.0 all-gather.20.cloned.1.call-start
  238.0 0.7 all-gather.20.cloned.1.call-update
  238.7 0.2 reduce-scatter.2.cloned.1.call-start
  238.9 0.0 copy-done.1
  238.9 0.0 copy-done.2
  239.0 82.7 %all-reduce.3.cloned.1.call-done = bf16[1024,2048]{1,0:T(8,128)(2,1)} async-done(((bf16[1024,2048]{1,0:T(8,128)(2,1)}), bf16[1024,2048]{1,0:T(8,128)(2,1)}) %all-reduce.3.cloned.1.call-update) | async-done | bytes 4194320 | tf_op jit(solution)/shard_map/psum | solution.py:63
  321.6 0.0 copy-start
  321.6 3.2 fusion
  324.9 0.2 copy-done
  325.1 5.3 fusion.2
  330.4 142.6 %all-gather.18.cloned.1.call-done = bf16[2048,2048]{1,0:T(8,128)(2,1)} async-done(((bf16[512,2048]{1,0:T(8,128)(2,1)}), bf16[2048,2048]{1,0:T(8,128)(2,1)}) %all-gather.18.cloned.1.call-update) | async-done | bytes 8388624 | tf_op jit(solution)/shard_map/all_gather | solution.py:69
  473.0 149.4 %all-gather.20.cloned.1.call-done = bf16[2048,2048]{1,0:T(8,128)(2,1)} async-done(((bf16[2048,512]{1,0:T(8,128)(2,1)}), bf16[2048,2048]{1,0:T(8,128)(2,1)}) %all-gather.20.cloned.1.call-update) | async-done | bytes 8388624 | tf_op jit(solution)/shard_map/all_gather | solution.py:75
  622.4 25.7 %fusion.18 = bf16[1024,2048]{1,0:T(8,128)(2,1)} fusion(bf16[2048,2048]{1,0:T(8,128)(2,1)} %all-gather.20.cloned.1.call-done, bf16[2048,2048]{1,0:T(8,128)(2,1)} %all-gather.18.cloned.1.call-done, bf16[1024,2048]{1,0:T(8,128)(2,1)} %get-tuple-element.6, f32[2048]{0:T(1024)S(1)} %convert_element_type.92, f32[1024]{0:T(1024)S(1)} %add_rsqrt_fusion.1), kind=kOutput, calls=%fused_computation.22 | convolution fusion | flops 17196646400 | bytes 25178112 | tf_op jit(solution)/shard_map/dot_general | solution.py:73
  648.1 0.0 reduce-scatter.2.cloned.1.call-update
  648.1 0.8 dynamic-slice_convert_fusion.1
  648.8 41.9 %reduce-scatter.2.cloned.1.call-done = bf16[1024,512]{1,0:T(8,128)(2,1)} async-done(((bf16[1024,2048]{1,0:T(8,128)(2,1)}), bf16[1024,512]{1,0:T(8,128)(2,1)}) %reduce-scatter.2.cloned.1.call-update) | async-done | bytes 1048592 | tf_op jit(solution)/shard_map/reduce_scatter | solution.py:78
  690.8 1.5 fusion.21
  692.3 5.8 psum.15
  698.1 3.0 fusion.24
  (7 shorter events, 0.0 us)
Async XLA Ops:
  6.5 39.6 %all-gather.8.cloned.1.call-start = ((), (), s32[]{:S(2)}) async-start(), calls=%async_computation.1 | async-start | bytes 5242880 | tf_op jit(solution)/shard_map/all_gather | solution.py:42
  7.3 86.1 %all-gather.12.cloned.1.call-start = ((), (), s32[]{:S(2)}) async-start(), calls=%async_computation.3 | async-start | bytes 2621440 | tf_op jit(solution)/shard_map/all_gather | solution.py:49
  8.0 131.4 %all-gather.14.cloned.1.call-start = ((), (), s32[]{:S(2)}) async-start(), calls=%async_computation.4 | async-start | bytes 2621440 | tf_op jit(solution)/shard_map/all_gather | solution.py:50
  8.7 176.6 %all-gather.10.cloned.1.call-start = ((), (), s32[]{:S(2)}) async-start(), calls=%async_computation.2 | async-start | bytes 2621440 | tf_op jit(solution)/shard_map/all_gather | solution.py:48
  9.3 221.9 %all-gather.16.cloned.1.call-start = ((), (), s32[]{:S(2)}) async-start(), calls=%async_computation.5 | async-start | bytes 2621440 | tf_op jit(solution)/shard_map/all_gather | solution.py:60
  9.9 311.7 %all-reduce.3.cloned.1.call-start = ((), (), s32[]{:S(2)}) async-start(), calls=%async_computation.6 | async-start | bytes 8388608 | tf_op jit(solution)/shard_map/psum | solution.py:63
  237.2 1.8 copy-start.1
  237.2 1.8 copy-start.2
  237.2 235.8 %all-gather.18.cloned.1.call-start = ((), (), s32[]{:S(2)}) async-start(), calls=%async_computation.7 | async-start | bytes 10485760 | tf_op jit(solution)/shard_map/all_gather | solution.py:69
  237.9 384.4 %all-gather.20.cloned.1.call-start = ((), (), s32[]{:S(2)}) async-start(), calls=%async_computation.8 | async-start | bytes 10485760 | tf_op jit(solution)/shard_map/all_gather | solution.py:75
  238.7 452.1 %reduce-scatter.2.cloned.1.call-start = ((), (), s32[]{:S(2)}) async-start(), calls=%async_computation.9 | async-start | bytes 5242880 | tf_op jit(solution)/shard_map/reduce_scatter | solution.py:78
  321.6 3.4 copy-start
Sparse Core Ops, SparseCore 0:
  8.9 37.1 all-gather.7
  47.7 45.6 all-gather.11
  94.9 44.4 all-gather.13
  140.9 44.4 all-gather.9
  186.8 44.4 all-gather.15
  237.3 84.2 all-reduce.2
  323.2 149.7 all-gather.17
  474.6 147.7 all-gather.19
  648.2 42.5 reduce-scatter.1
where the time goes:
time: 708 us
  waiting for transfers between devices  622 us (88%)
  matrix products  47.3 us (7%)
  other arithmetic  18.9 us (3%)
  between operations  13.3 us (2%)
    all_gather x1, waiting for transfers between devices, body(): lax.all_gather(down_weight, 'fs', axis=1, tiled=True)  149 us
    all_gather x1, waiting for transfers between devices, body(): lax.all_gather(up_weight, 'fs', axis=0, tiled=True)  143 us
    psum x1, waiting for transfers between devices, body(): mixed = lax.psum(partial_mix.astype(jnp.bfloat16), 'tp').astype(jnp.float32)  82.7 us
    all_gather x1, waiting for transfers between devices, body(): cgate = add_rows(lax.all_gather(cgate_weight, 'fs', axis=0, tiled=True))  44.2 us
    reduce_scatter x1, waiting for transfers between devices, body(): lax.psum_scatter(partial_ffn.astype(jnp.bfloat16), 'tp', scatter_dimensio...  41.9 us
    all_gather x1, waiting for transfers between devices, body(): value = add_rows(lax.all_gather(value_weight, 'fs', axis=0, tiled=True))  40.8 us
    all_gather x1, waiting for transfers between devices, body(): lax.all_gather(out_weight, 'fs', axis=1, tiled=True)  40.7 us
    all_gather x1, waiting for transfers between devices, body(): bgate = add_rows(lax.all_gather(bgate_weight, 'fs', axis=0, tiled=True))  40 us
  transfers between devices with their start and end apart: 9, of which 9 were waited for; matrix products, arithmetic and copies ran while one was open for 4% of the time, Pallas kernels for 0%

commit v1 on v0

--- a/solution.py
+++ b/solution.py
@@ -72,7 +72,7 @@
     active = jnp.square(jnp.maximum(lifted, 0.0)).astype(jnp.bfloat16)
     partial_ffn = jnp.dot(
         active,
-        lax.all_gather(down_weight, "fs", axis=1, tiled=True),
+        jnp.concatenate(lax.all_gather(down_weight, "fs"), axis=1),
         preferred_element_type=jnp.float32,
     )
     ffn = lax.psum_scatter(

time: 708 us -> 708 us (level)
  waiting for transfers between devices: 622 us -> 610 us
  local copies, waits for them, and re-layouts: 0.23 us -> 12 us
    reshape x0 -> x1, local copies, waits for them, and re-layouts: none -> 11.8 us  [body(): jnp.concatenate(lax.all_gather(down_weight, 'fs'), axis=1)]
  transfers between devices with their start and end apart: 9 -> 9, of which waited for: 9 -> 9; matrix products, arithmetic and copies ran while one was open for 4% -> 6% of each run, Pallas kernels for 0% -> 0%
where the time goes in v1:
time: 708 us
  waiting for transfers between devices  610 us (86%)
  matrix products  47.3 us (7%)
  other arithmetic  18.9 us (3%)
  between operations  13.3 us (2%)
  local copies, waits for them, and re-layouts  12 us (2%)
    all_gather x1, waiting for transfers between devices, body(): lax.all_gather(down_weight, 'fs')  143 us
    all_gather x1, waiting for transfers between devices, body(): lax.all_gather(up_weight, 'fs', axis=0, tiled=True)  138 us
    psum x1, waiting for transfers between devices, body(): mixed = lax.psum(partial_mix.astype(jnp.bfloat16), 'tp').astype(jnp.float32)  82.7 us
    all_gather x1, waiting for transfers between devices, body(): cgate = add_rows(lax.all_gather(cgate_weight, 'fs', axis=0, tiled=True))  44.2 us
    reduce_scatter x1, waiting for transfers between devices, body(): lax.psum_scatter(partial_ffn.astype(jnp.bfloat16), 'tp', scatter_dimensio...  42 us
    all_gather x1, waiting for transfers between devices, body(): value = add_rows(lax.all_gather(value_weight, 'fs', axis=0, tiled=True))  40.8 us
    all_gather x1, waiting for transfers between devices, body(): lax.all_gather(out_weight, 'fs', axis=1, tiled=True)  40.7 us
    all_gather x1, waiting for transfers between devices, body(): bgate = add_rows(lax.all_gather(bgate_weight, 'fs', axis=0, tiled=True))  40 us
  transfers between devices with their start and end apart: 9, of which 9 were waited for; matrix products, arithmetic and copies ran while one was open for 6% of the time, Pallas kernels for 0%

profile of v1, /device:TPU:0, one launch (start us, length us, event | category | flops | bytes accessed | tf_op | source)
XLA Modules:
  0.0 707.6 jit_solution(8327947060965505404)
XLA Ops:
  6.5 0.0 all-gather.9.cloned.1.call-start
  6.5 0.7 all-gather.9.cloned.1.call-update
  7.3 0.0 all-gather.13.cloned.1.call-start
  7.3 0.7 all-gather.13.cloned.1.call-update
  8.0 0.0 all-gather.15.cloned.1.call-start
  8.1 0.7 all-gather.15.cloned.1.call-update
  8.7 0.0 all-gather.11.cloned.1.call-start
  8.8 0.5 all-gather.11.cloned.1.call-update
  9.3 0.0 all-gather.17.cloned.1.call-start
  9.4 0.5 all-gather.17.cloned.1.call-update
  9.9 0.0 all-reduce.3.cloned.1.call-start
  10.0 0.7 dynamic-slice_convert_fusion
  10.7 0.7 convert_element_type.76
  11.4 34.8 %all-gather.9.cloned.1.call-done = bf16[1024,2048]{1,0:T(8,128)(2,1)} async-done(((bf16[1024,512]{1,0:T(8,128)(2,1)}), bf16[1024,2048]{1,0:T(8,128)(2,1)}) %all-gather.9.cloned.1.call-update) | async-done | bytes 4194320 | tf_op jit(solution)/shard_map/all_gather | solution.py:42
  46.1 3.1 fusion.5
  49.2 44.2 %all-gather.13.cloned.1.call-done = bf16[2048,512]{1,0:T(8,128)(2,1)} async-done(((bf16[512,512]{1,0:T(8,128)(2,1)}), bf16[2048,512]{1,0:T(8,128)(2,1)}) %all-gather.13.cloned.1.call-update) | async-done | bytes 2097168 | tf_op jit(solution)/shard_map/all_gather | solution.py:49
  93.4 5.2 convolution_convert_fusion.2
  98.6 40.8 %all-gather.15.cloned.1.call-done = bf16[2048,512]{1,0:T(8,128)(2,1)} async-done(((bf16[512,512]{1,0:T(8,128)(2,1)}), bf16[2048,512]{1,0:T(8,128)(2,1)}) %all-gather.15.cloned.1.call-update) | async-done | bytes 2097168 | tf_op jit(solution)/shard_map/all_gather | solution.py:50
  139.4 5.2 convert_multiply_fusion.8
  144.7 0.6 multiply_add_fusion
  145.3 40.0 %all-gather.11.cloned.1.call-done = bf16[2048,512]{1,0:T(8,128)(2,1)} async-done(((bf16[512,512]{1,0:T(8,128)(2,1)}), bf16[2048,512]{1,0:T(8,128)(2,1)}) %all-gather.11.cloned.1.call-update) | async-done | bytes 2097168 | tf_op jit(solution)/shard_map/all_gather | solution.py:48
  185.4 5.2 fusion.25
  190.6 40.7 %all-gather.17.cloned.1.call-done = bf16[512,2048]{1,0:T(8,128)(2,1)} async-done(((bf16[512,512]{1,0:T(8,128)(2,1)}), bf16[512,2048]{1,0:T(8,128)(2,1)}) %all-gather.17.cloned.1.call-update) | async-done | bytes 2097168 | tf_op jit(solution)/shard_map/all_gather | solution.py:60
  231.3 5.9 convolution_convert_fusion
  237.2 0.0 copy-start.1
  237.2 0.0 copy-start.2
  237.2 0.0 all-reduce.3.cloned.1.call-update
  237.2 0.0 all-gather.21.cloned.1.call-start
  237.2 0.7 all-gather.21.cloned.1.call-update
  237.9 0.0 all-gather.19.cloned.1.call-start
  238.0 0.7 all-gather.19.cloned.1.call-update
  238.7 0.2 reduce-scatter.2.cloned.1.call-start
  238.9 0.0 copy-done.1
  238.9 0.0 copy-done.2
  239.0 82.7 %all-reduce.3.cloned.1.call-done = bf16[1024,2048]{1,0:T(8,128)(2,1)} async-done(((bf16[1024,2048]{1,0:T(8,128)(2,1)}), bf16[1024,2048]{1,0:T(8,128)(2,1)}) %all-reduce.3.cloned.1.call-update) | async-done | bytes 4194320 | tf_op jit(solution)/shard_map/psum | solution.py:63
  321.6 3.2 fusion
  324.9 0.2 copy-done
  325.1 5.3 fusion.2
  330.4 142.6 %all-gather.21.cloned.1.call-done = bf16[8192,512]{1,0:T(8,128)(2,1)} async-done(((bf16[2048,512]{1,0:T(8,128)(2,1)}), bf16[8192,512]{1,0:T(8,128)(2,1)}) %all-gather.21.cloned.1.call-update) | async-done | bytes 8388624 | tf_op jit(solution)/shard_map/all_gather | solution.py:75
  473.0 11.8 %copy.13 = bf16[2048,4,512]{0,2,1:T(8,128)(2,1)} copy(bf16[2048,4,512]{2,0,1:T(8,128)(2,1)} %bitcast.19) | data formatting | bytes 16777216 | tf_op jit(solution)/shard_map/reshape | solution.py:75
  484.8 137.6 %all-gather.19.cloned.1.call-done = bf16[2048,2048]{1,0:T(8,128)(2,1)} async-done(((bf16[512,2048]{1,0:T(8,128)(2,1)}), bf16[2048,2048]{1,0:T(8,128)(2,1)}) %all-gather.19.cloned.1.call-update) | async-done | bytes 8388624 | tf_op jit(solution)/shard_map/all_gather | solution.py:69
  622.4 25.6 %fusion.18 = bf16[1024,2048]{1,0:T(8,128)(2,1)} fusion(bf16[2048,2048]{0,1:T(8,128)(2,1)} %bitcast.20, bf16[2048,2048]{1,0:T(8,128)(2,1)} %all-gather.19.cloned.1.call-done, bf16[1024,2048]{1,0:T(8,128)(2,1)} %get-tuple-element.6, f32[2048]{0:T(1024)S(1)} %convert_element_type.92, f32[1024]{0:T(1024)S(1)} %add_rsqrt_fusion.1), kind=kOutput, calls=%fused_computation.22 | convolution fusion | flops 17196646400 | bytes 25178112 | tf_op jit(solution)/shard_map/dot_general | solution.py:73
  648.0 0.0 reduce-scatter.2.cloned.1.call-update
  648.0 0.8 dynamic-slice_convert_fusion.1
  648.8 42.0 %reduce-scatter.2.cloned.1.call-done = bf16[1024,512]{1,0:T(8,128)(2,1)} async-done(((bf16[1024,2048]{1,0:T(8,128)(2,1)}), bf16[1024,512]{1,0:T(8,128)(2,1)}) %reduce-scatter.2.cloned.1.call-update) | async-done | bytes 1048592 | tf_op jit(solution)/shard_map/reduce_scatter | solution.py:78
  690.8 1.5 fusion.21
  692.3 5.8 psum.15
  698.1 3.0 fusion.24
  (8 shorter events, 0.0 us)
Async XLA Ops:
  6.5 39.6 %all-gather.9.cloned.1.call-start = ((), (), s32[]{:S(2)}) async-start(), calls=%async_computation.1 | async-start | bytes 5242880 | tf_op jit(solution)/shard_map/all_gather | solution.py:42
  7.3 86.1 %all-gather.13.cloned.1.call-start = ((), (), s32[]{:S(2)}) async-start(), calls=%async_computation.3 | async-start | bytes 2621440 | tf_op jit(solution)/shard_map/all_gather | solution.py:49
  8.0 131.4 %all-gather.15.cloned.1.call-start = ((), (), s32[]{:S(2)}) async-start(), calls=%async_computation.4 | async-start | bytes 2621440 | tf_op jit(solution)/shard_map/all_gather | solution.py:50
  8.7 176.6 %all-gather.11.cloned.1.call-start = ((), (), s32[]{:S(2)}) async-start(), calls=%async_computation.2 | async-start | bytes 2621440 | tf_op jit(solution)/shard_map/all_gather | solution.py:48
  9.3 221.9 %all-gather.17.cloned.1.call-start = ((), (), s32[]{:S(2)}) async-start(), calls=%async_computation.5 | async-start | bytes 2621440 | tf_op jit(solution)/shard_map/all_gather | solution.py:60
  9.9 311.7 %all-reduce.3.cloned.1.call-start = ((), (), s32[]{:S(2)}) async-start(), calls=%async_computation.6 | async-start | bytes 8388608 | tf_op jit(solution)/shard_map/psum | solution.py:63
  237.2 1.8 copy-start.1
  237.2 1.8 copy-start.2
  237.2 235.8 %all-gather.21.cloned.1.call-start = ((), (), s32[]{:S(2)}) async-start(), calls=%async_computation.9 | async-start | bytes 10485760 | tf_op jit(solution)/shard_map/all_gather | solution.py:75
  237.9 384.4 %all-gather.19.cloned.1.call-start = ((), (), s32[]{:S(2)}) async-start(), calls=%async_computation.7 | async-start | bytes 10485760 | tf_op jit(solution)/shard_map/all_gather | solution.py:69
  238.7 452.1 %reduce-scatter.2.cloned.1.call-start = ((), (), s32[]{:S(2)}) async-start(), calls=%async_computation.8 | async-start | bytes 5242880 | tf_op jit(solution)/shard_map/reduce_scatter | solution.py:78
  321.6 3.4 copy-start
Sparse Core Ops, SparseCore 0:
  8.9 37.1 all-gather.8
  47.7 45.6 all-gather.12
  94.9 44.4 all-gather.14
  140.9 44.4 all-gather.10
  186.8 44.4 all-gather.16
  237.3 84.2 all-reduce.2
  323.2 149.7 all-gather.20
  474.6 147.7 all-gather.18
  648.1 42.6 reduce-scatter.1
